TPU v7x, 512 devices: a whole 4x8x8 slice. The times are simulated.
512 devices in a mesh: kv: 64 (over z, y), tp: 8 (over x, core).
Axes of the slice: x: 4, y: 8, z: 8, core: 2. Of those that a mesh axis runs over, the one named last changes fastest.
Arguments:
- queries: bfloat16 [8192, 1024], P('kv', 'tp'), may hold values from -4 to 4
- keys: bfloat16 [8192, 1024], P('kv', 'tp'), may hold values from -4 to 4
- values: bfloat16 [8192, 1024], P('kv', 'tp'), may hold values from -4 to 4
- cotangent: bfloat16 [8192, 1024], P('kv', 'tp'), may hold values from -4 to 4
- log_sum: float32 [16, 8192], P('tp', 'kv'), may hold values from 4.5 to 7.5
- chosen: int32 [16, 256, 12], P('tp'), may hold values from 0 to 255, as said below
- normed_input: bfloat16 [8192, 2048], P('kv', 'tp'), may hold values from -0.0625 to 0.0625
Outputs:
- grad_queries: bfloat16 [8192, 1024], P('kv', 'tp')
- grad_keys: bfloat16 [8192, 1024], P('kv', 'tp')
- grad_values: bfloat16 [8192, 1024], P('kv', 'tp')
- grad_weight: float32 [2048, 1024], P('kv', 'tp')
Inputs may be any that keep to these rules, and one draw needn't show every extreme that they name: `chosen`: for each head, the distinct blocks below their own query block that the query blocks of one device's 128 positions choose include at most 1 block of any one device's span of 128 positions, and exactly 1 for some pairs of devices. Within one list the entries below the query block's own index are distinct.
All inputs are finite; a program needn't handle non-finite values.
Results may differ from a plain program's by a relative error of at most 0.0085.
Values may be sent and summed in bfloat16 or wider, within the bound.
A program may use at most 64 MiB of HBM per device.

v0:
```python
import jax
import jax.numpy as jnp
from jax import lax
from jax.sharding import PartitionSpec as P

HD = 64
BLK = 32
SEL = 12
MOST = 1
MASKED = -1e30


def sent_together(arrays, axis, split_dim, concat_dim, along):
    both = jnp.concatenate(arrays, axis=along)
    whole, at, finished = (
        lax.all_to_all(both, axis, split_axis=split_dim, concat_axis=concat_dim, tiled=True),
        0,
        [],
    )
    for a in arrays:
        finished.append(lax.slice_in_dim(whole, at, at + a.shape[along], axis=along))
        at += a.shape[along]
    return tuple(finished)


def split_up(array, dim, size):
    dims = array.shape
    tiles = array.reshape(*dims[:dim], size, dims[dim] // size, *dims[dim + 1 :])
    return jnp.moveaxis(tiles, dim, 0)


def sum_at_owner(array, axis, dim):
    tiles = split_up(array, dim, lax.axis_size(axis))
    arrived = lax.all_to_all(tiles, axis, split_axis=0, concat_axis=0, tiled=True)
    return arrived.astype(jnp.float32).sum(axis=0)


def slot_picks(needed):
    span_width = needed.shape[-1]
    counted = needed.astype(jnp.int32)
    before = jnp.cumsum(counted, axis=-1) - counted
    places = jnp.arange(span_width, dtype=jnp.int32)
    picked, present = ([], [])
    hitting = needed & (before == 0)
    present.append(jnp.any(hitting, axis=-1))
    picked.append(jnp.sum(jnp.where(hitting, places, 0), axis=-1))
    return (jnp.stack(picked, axis=-1), jnp.stack(present, axis=-1))


def to_blocks(row_block, tok_rows, head_count):
    shards = row_block.shape[0] // tok_rows
    shaped = row_block.reshape(shards, tok_rows // BLK, BLK, head_count, HD).transpose(
        0, 3, 1, 2, 4
    )
    return shaped.reshape(shards * head_count * (tok_rows // BLK), BLK * HD)


def heads_from(row_block, head_count):
    blocks_dev = row_block.shape[0] // BLK
    return row_block.reshape(blocks_dev, BLK, head_count, HD).transpose(2, 0, 1, 3)


def back_rows(blocked):
    head_count, blocks_dev = (blocked.shape[0], blocked.shape[1])
    return blocked.transpose(1, 2, 0, 3).reshape(blocks_dev * BLK, head_count * HD)


def body(queries, keys, values, cotangent, log_sum, chosen, normed_input):
    tok_rows = queries.shape[0]
    head_count = log_sum.shape[0]
    blocks_dev = tok_rows // BLK
    devices = lax.axis_size("kv")
    my_index = lax.axis_index("kv")
    block_total = chosen.shape[1]
    tile_size = BLK * HD
    score_scale = HD ** (-0.5)
    places = jnp.arange(blocks_dev, dtype=jnp.int32)
    own_ids = my_index * blocks_dev + places
    my_lists = lax.dynamic_slice_in_dim(chosen, my_index * blocks_dev, blocks_dev, 1)
    usable = my_lists < own_ids[None, :, None]
    every_block = jnp.arange(block_total, dtype=jnp.int32)
    need_here = jnp.any((my_lists[..., None] == every_block) & usable[..., None], axis=(1, 2))
    req_picked, req_present = slot_picks(need_here.reshape(head_count, devices, blocks_dev))
    grouped = chosen.reshape(head_count, devices, blocks_dev, SEL)
    row_ids = every_block.reshape(devices, blocks_dev)
    usable_all = grouped < row_ids[None, :, :, None]
    need_there = jnp.any((grouped[..., None] == own_ids) & usable_all[..., None], axis=(2, 3))
    own_picked, own_present = slot_picks(need_there)
    own_picked = own_picked.transpose(1, 0, 2)
    own_present = own_present.transpose(1, 0, 2)
    head_base = (jnp.arange(head_count, dtype=jnp.int32) * blocks_dev)[None, :, None]
    send_ids = (head_base + own_picked).reshape(-1)
    key_send = jnp.take(to_blocks(keys, tok_rows, head_count), send_ids, axis=0).reshape(
        devices, head_count, MOST, tile_size
    )
    value_send = jnp.take(to_blocks(values, tok_rows, head_count), send_ids, axis=0).reshape(
        devices, head_count, MOST, tile_size
    )
    key_tiles, value_tiles = sent_together((key_send, value_send), "kv", 0, 0, 1)
    owners = my_lists // blocks_dev
    local_ids = my_lists % blocks_dev
    head_ids = jnp.arange(head_count, dtype=jnp.int32)[:, None, None]
    rows_at = (head_ids * devices + owners).reshape(-1)
    slot_at = jnp.take(req_picked.reshape(head_count * devices, MOST), rows_at, axis=0).reshape(
        head_count, blocks_dev, SEL, MOST
    )
    slot_live = jnp.take(req_present.reshape(head_count * devices, MOST), rows_at, axis=0).reshape(
        head_count, blocks_dev, SEL, MOST
    )
    matches = (slot_at == local_ids[..., None]) & slot_live
    slot_of = jnp.sum(jnp.where(matches, jnp.arange(MOST, dtype=jnp.int32), 0), axis=-1)
    tile_ids = jnp.where(usable, (owners * head_count + head_ids) * MOST + slot_of, 0).reshape(-1)
    sel_keys = jnp.take(key_tiles.reshape(-1, tile_size), tile_ids, axis=0).reshape(
        head_count, blocks_dev, SEL * BLK, HD
    )
    sel_values = jnp.take(value_tiles.reshape(-1, tile_size), tile_ids, axis=0).reshape(
        head_count, blocks_dev, SEL * BLK, HD
    )
    keys_all = jnp.concatenate([sel_keys, heads_from(keys, head_count)], axis=2)
    values_all = jnp.concatenate([sel_values, heads_from(values, head_count)], axis=2)
    causal = jnp.arange(BLK)[:, None] >= jnp.arange(BLK)[None, :]
    sel_mask = jnp.broadcast_to(
        jnp.repeat(usable, BLK, axis=2)[:, :, None, :], (head_count, blocks_dev, BLK, SEL * BLK)
    )
    allowed = jnp.concatenate(
        [sel_mask, jnp.broadcast_to(causal, (head_count, blocks_dev, BLK, BLK))], axis=3
    )
    q_blocks = heads_from(queries, head_count)
    g_blocks = heads_from(cotangent, head_count)
    log_rows = log_sum.reshape(head_count, blocks_dev, BLK)[..., None]
    scores = (
        jnp.einsum("hiqd,hikd->hiqk", q_blocks, keys_all, preferred_element_type=jnp.float32)
        * score_scale
    )
    weights = jnp.exp(jnp.where(allowed, scores - log_rows, MASKED))
    value_dots = jnp.einsum(
        "hiqd,hikd->hiqk", g_blocks, values_all, preferred_element_type=jnp.float32
    )
    row_delta = jnp.sum(weights * value_dots, axis=-1, keepdims=True)
    score_grad = (weights * (value_dots - row_delta)).astype(jnp.bfloat16)
    weights_low = weights.astype(jnp.bfloat16)
    query_grad = (
        jnp.einsum("hiqk,hikd->hiqd", score_grad, keys_all, preferred_element_type=jnp.float32)
        * score_scale
    )
    key_grad = (
        jnp.einsum("hiqk,hiqd->hikd", score_grad, q_blocks, preferred_element_type=jnp.float32)
        * score_scale
    )
    value_grad = jnp.einsum(
        "hiqk,hiqd->hikd", weights_low, g_blocks, preferred_element_type=jnp.float32
    )
    grad_queries = back_rows(query_grad).astype(jnp.bfloat16)

    def to_slots(gradient):
        chosen_part = gradient[:, :, : SEL * BLK].reshape(-1, tile_size)
        slotted = jax.ops.segment_sum(
            chosen_part, tile_ids, num_segments=devices * head_count * MOST
        )
        return slotted.reshape(devices, head_count, MOST, tile_size)

    back_keys, back_values = (
        lax.all_to_all(
            to_slots(key_grad).astype(jnp.bfloat16), "kv", split_axis=0, concat_axis=0, tiled=True
        ).astype(jnp.float32),
        lax.all_to_all(
            to_slots(value_grad).astype(jnp.bfloat16), "kv", split_axis=0, concat_axis=0, tiled=True
        ).astype(jnp.float32),
    )
    land_ids = jnp.where(own_present, head_base + own_picked, head_count * blocks_dev).reshape(-1)

    def settle(returned, gradient):
        flat_tiles = returned.reshape(-1, tile_size)
        targets = (
            jnp.arange(head_count * blocks_dev, dtype=jnp.int32)[:, None] == land_ids[None, :]
        ).astype(jnp.float32)
        landed = jnp.dot(
            targets, flat_tiles, precision=lax.Precision.HIGHEST, preferred_element_type=jnp.float32
        )
        summed = landed.reshape(head_count, blocks_dev, BLK, HD) + gradient[:, :, SEL * BLK :]
        return back_rows(summed).astype(jnp.bfloat16)

    grad_keys = settle(back_keys, key_grad)
    grad_values = settle(back_values, value_grad)
    whole_input = lax.all_gather(normed_input, "tp", axis=1, tiled=True)
    grad_weight = sum_at_owner(
        lax.dot_general(
            whole_input, grad_queries, (((0,), (0,)), ((), ())), preferred_element_type=jnp.float32
        ).astype(jnp.bfloat16),
        "kv",
        0,
    )
    return (grad_queries, grad_keys, grad_values, grad_weight)


def solution(mesh):
    in_specs = (
        P("kv", "tp"),
        P("kv", "tp"),
        P("kv", "tp"),
        P("kv", "tp"),
        P("tp", "kv"),
        P("tp", None, None),
        P("kv", "tp"),
    )
    out_specs = (P("kv", "tp"), P("kv", "tp"), P("kv", "tp"), P("kv", "tp"))
    return jax.shard_map(body, mesh=mesh, in_specs=in_specs, out_specs=out_specs, check_vma=False)
```

profile of v0, /device:TPU:8, one launch (start us, length us, event | category | flops | bytes accessed | tf_op | source)
XLA Modules:
  0.0 145.6 jit_solution(14934738471255190425)
XLA Ops:
  0.7 0.9 copy.75
  2.6 0.8 reshape.213
  3.9 0.9 gather_fusion
  4.8 0.9 gather_fusion.1
  6.0 0.3 reshape.219
  6.3 0.3 reshape.216
  6.6 2.1 %pad_maximum_fusion = bf16[64,4,1,2048]{3,1,2,0:T(4,128)(2,1)} fusion(bf16[64,2,1,2048]{3,1,2,0:T(2,128)(2,1)S(1)} %bitcast.101, bf16[64,2,1,2048]{3,1,2,0:T(2,128)(2,1)S(1)} %bitcast.102), kind=kLoop, calls=%fused_computation.18 | loop fusion | flops 2097152 | bytes 2097152 | tf_op jit(solution)/shard_map/concatenate | solution.py:14
  8.7 16.7 %all-to-all-start = ((bf16[64,4,1,2048]{3,1,2,0:T(4,128)(2,1)}), bf16[64,4,1,2048]{3,1,2,0:T(4,128)(2,1)S(1)}, u32[]{:S(2)}, u32[]{:S(2)}) async-start(bf16[64,4,1,2048]{3,1,2,0:T(4,128)(2,1)} %pad_maximum_fusion), calls=%async_computation | async-start | bytes 2097152 | tf_op jit(solution)/shard_map/all_to_all | solution.py:16
  26.9 27.8 %all-to-all-done = bf16[64,4,1,2048]{3,1,2,0:T(4,128)(2,1)S(1)} async-done(((bf16[64,4,1,2048]{3,1,2,0:T(4,128)(2,1)}), bf16[64,4,1,2048]{3,1,2,0:T(4,128)(2,1)S(1)}, u32[]{:S(2)}, u32[]{:S(2)}) %all-to-all-start) | async-done | bytes 1048608 | tf_op jit(solution)/shard_map/all_to_all | solution.py:16
  54.7 0.7 fusion.46
  55.9 0.8 gather_fusion.3
  56.7 0.8 gather_fusion.2
  57.7 0.8 reshape.226
  58.5 0.3 copy.87
  58.8 0.8 reshape.222
  59.6 0.3 copy.84
  60.2 0.4 multiply_reduce_fusion
  60.8 0.3 convolution_multiply_fusion
  61.2 0.3 copy-done.1
  61.7 0.5 copy.91
  62.1 0.5 reshape.270
  62.6 2.0 %scatter_custom_fusion = f32[128,2048]{1,0:T(8,128)S(1)} fusion(s32[96]{0:T(128)S(1)} %reshape.221, f32[96,2048]{1,0:T(8,128)S(1)} %reshape.270, f32[]{:T(128)} %constant.105.clone.1), kind=kCustom, calls=%fused_computation.26 | custom fusion | flops 196608 | bytes 1048580 | tf_op jit(solution)/shard_map/scatter-add | solution.py:157
  64.7 1.2 convert_element_type.84
  65.9 7.1 %all-to-all-start.1 = ((bf16[64,2,1,2048]{3,1,2,0:T(2,128)(2,1)}), bf16[64,2,1,2048]{3,1,2,0:T(2,128)(2,1)}, u32[]{:S(2)}, u32[]{:S(2)}) async-start(bf16[64,2,1,2048]{3,1,2,0:T(2,128)(2,1)} %bitcast.18), calls=%async_computation.1 | async-start | bytes 1048576 | tf_op jit(solution)/shard_map/all_to_all | solution.py:163
  73.1 0.3 fusion.16
  73.4 1.0 copy-done
  74.4 0.5 copy.96
  74.9 0.5 reshape.278
  75.4 2.0 %scatter_custom_fusion.1 = f32[128,2048]{1,0:T(8,128)S(1)} fusion(s32[96]{0:T(128)S(1)} %reshape.221, f32[96,2048]{1,0:T(8,128)S(1)} %reshape.278, f32[]{:T(128)} %constant.105.clone.1), kind=kCustom, calls=%fused_computation.24 | custom fusion | flops 196608 | bytes 1048580 | tf_op jit(solution)/shard_map/scatter-add | solution.py:157
  77.6 1.1 convert_element_type.90
  78.7 12.8 %all-to-all-done.1 = bf16[64,2,1,2048]{3,1,2,0:T(2,128)(2,1)} async-done(((bf16[64,2,1,2048]{3,1,2,0:T(2,128)(2,1)}), bf16[64,2,1,2048]{3,1,2,0:T(2,128)(2,1)}, u32[]{:S(2)}, u32[]{:S(2)}) %all-to-all-start.1) | async-done | bytes 524320 | tf_op jit(solution)/shard_map/all_to_all | solution.py:163
  91.5 5.4 %all-to-all-start.2 = ((bf16[64,2,1,2048]{3,1,2,0:T(2,128)(2,1)}), bf16[64,2,1,2048]{3,1,2,0:T(2,128)(2,1)S(1)}, u32[]{:S(2)}, u32[]{:S(2)}) async-start(bf16[64,2,1,2048]{3,1,2,0:T(2,128)(2,1)} %bitcast.24), calls=%async_computation.2 | async-start | bytes 1048576 | tf_op jit(solution)/shard_map/all_to_all | solution.py:166
  97.2 13.5 %all_gather.3 = bf16[128,2048]{1,0:T(8,128)(2,1)S(1)} all-gather(bf16[128,256]{1,0:T(8,128)(2,1)S(1)} %copy-done.12), channel_id=1, replica_groups=mesh['kv'=64,'tp'=8] {'tp'}, dimensions={1}, use_global_device_ids=true | all-gather | bytes 589824 | tf_op jit(solution)/shard_map/all_gather | solution.py:185
  110.6 0.3 fusion.6
  111.1 0.3 fusion
  111.4 1.0 copy.101
  112.4 2.6 %all-to-all-done.2 = bf16[64,2,1,2048]{3,1,2,0:T(2,128)(2,1)S(1)} async-done(((bf16[64,2,1,2048]{3,1,2,0:T(2,128)(2,1)}), bf16[64,2,1,2048]{3,1,2,0:T(2,128)(2,1)S(1)}, u32[]{:S(2)}, u32[]{:S(2)}) %all-to-all-start.2) | async-done | bytes 524320 | tf_op jit(solution)/shard_map/all_to_all | solution.py:166
  115.0 10.1 %all-to-all-start.3 = ((bf16[64,32,128]{2,1,0:T(8,128)(2,1)}), bf16[64,32,128]{2,1,0:T(8,128)(2,1)S(1)}, u32[]{:S(2)}, u32[]{:S(2)}) async-start(bf16[64,32,128]{2,1,0:T(8,128)(2,1)} %bitcast.30), calls=%async_computation.3 | async-start | bytes 1048576 | tf_op jit(solution)/shard_map/all_to_all | solution.py:34
  125.2 1.2 reshape.230
  126.4 0.3 copy.93
  126.7 0.5 fusion.31
  127.6 0.7 convert_element_type.87
  128.5 0.3 copy.98
  128.7 0.5 fusion.29
  129.4 1.0 fusion.19
  130.5 0.7 convert_element_type.93
  131.3 13.6 %all-to-all-done.3 = bf16[64,32,128]{2,1,0:T(8,128)(2,1)S(1)} async-done(((bf16[64,32,128]{2,1,0:T(8,128)(2,1)}), bf16[64,32,128]{2,1,0:T(8,128)(2,1)S(1)}, u32[]{:S(2)}, u32[]{:S(2)}) %all-to-all-start.3) | async-done | bytes 524320 | tf_op jit(solution)/shard_map/all_to_all | solution.py:34
  144.9 0.7 convert_reduce_fusion
  (94 shorter events, 5.5 us)
Async XLA Ops:
  0.6 3.0 %copy-start.7 = (bf16[128,128]{1,0:T(8,128)(2,1)S(1)}, bf16[128,128]{1,0:T(8,128)(2,1)}, u32[]{:S(2)}) copy-start(bf16[128,128]{1,0:T(8,128)(2,1)} %param.13) | copy-start | bytes 98308
  8.7 16.9 %copy-start.8 = (bf16[128,128]{1,0:T(8,128)(2,1)S(1)}, bf16[128,128]{1,0:T(8,128)(2,1)}, u32[]{:S(2)}) copy-start(bf16[128,128]{1,0:T(8,128)(2,1)} %param.12) | copy-start | bytes 98308
  8.7 17.1 %copy-start.13 = (s32[2,256,12]{1,0,2:T(2,128)S(1)}, s32[2,256,12]{1,0,2:T(2,128)}, u32[]{:S(2)}) copy-start(s32[2,256,12]{1,0,2:T(2,128)} %param.16) | copy-start | bytes 73732
  8.7 17.4 %copy-start.14 = (bf16[128,128]{1,0:T(8,128)(2,1)S(1)}, bf16[128,128]{1,0:T(8,128)(2,1)}, u32[]{:S(2)}) copy-start(bf16[128,128]{1,0:T(8,128)(2,1)} %param.14) | copy-start | bytes 98308
  8.7 17.5 %copy-start.16 = (f32[2,128]{1,0:T(2,128)S(1)}, f32[2,128]{1,0:T(2,128)}, u32[]{:S(2)}) copy-start(f32[2,128]{1,0:T(2,128)} %param.15) | copy-start | bytes 3076
  8.7 17.7 %copy-start.15 = (bf16[128,128]{1,0:T(8,128)(2,1)S(1)}, bf16[128,128]{1,0:T(8,128)(2,1)}, u32[]{:S(2)}) copy-start(bf16[128,128]{1,0:T(8,128)(2,1)} %param.11) | copy-start | bytes 98308
  8.7 46.0 %all-to-all-start = ((bf16[64,4,1,2048]{3,1,2,0:T(4,128)(2,1)}), bf16[64,4,1,2048]{3,1,2,0:T(4,128)(2,1)S(1)}, u32[]{:S(2)}, u32[]{:S(2)}) async-start(bf16[64,4,1,2048]{3,1,2,0:T(4,128)(2,1)} %pad_maximum_fusion), calls=%async_computation | async-start | bytes 2097152 | tf_op jit(solution)/shard_map/all_to_all | solution.py:16
  26.4 33.8 %copy-start.10 = (bf16[4,32,2,64]{1,3,0,2:T(8,128)(2,1)}, bf16[4,32,2,64]{1,3,0,2:T(8,128)(2,1)S(1)}, u32[]{:S(2)}) copy-start(bf16[4,32,2,64]{1,3,0,2:T(8,128)(2,1)S(1)} %copy.83) | copy-start | bytes 98308
  59.9 0.8 copy-start.5
  60.7 0.8 copy-start.1
  60.8 0.8 copy-start.3
  64.7 8.4 %copy-start.2 = (f32[2,4,32,416]{3,2,1,0:T(8,128)S(1)}, f32[2,4,32,416]{3,2,1,0:T(8,128)}, u32[]{:S(2)}) copy-start(f32[2,4,32,416]{3,2,1,0:T(8,128)} %copy-done.1) | copy-start | bytes 1277956
  65.9 25.6 %all-to-all-start.1 = ((bf16[64,2,1,2048]{3,1,2,0:T(2,128)(2,1)}), bf16[64,2,1,2048]{3,1,2,0:T(2,128)(2,1)}, u32[]{:S(2)}, u32[]{:S(2)}) async-start(bf16[64,2,1,2048]{3,1,2,0:T(2,128)(2,1)} %bitcast.18), calls=%async_computation.1 | async-start | bytes 1048576 | tf_op jit(solution)/shard_map/all_to_all | solution.py:163
  73.4 1.0 copy-start
  77.4 19.7 %copy-start.12 = (bf16[128,256]{1,0:T(8,128)(2,1)S(1)}, bf16[128,256]{1,0:T(8,128)(2,1)}, u32[]{:S(2)}) copy-start(bf16[128,256]{1,0:T(8,128)(2,1)} %param.17) | copy-start | bytes 196612
  77.5 33.1 %copy-start.4 = (bf16[2,4,32,416]{3,2,1,0:T(8,128)(2,1)S(1)}, bf16[2,4,32,416]{3,2,1,0:T(8,128)(2,1)}, u32[]{:S(2)}) copy-start(bf16[2,4,32,416]{3,2,1,0:T(8,128)(2,1)} %copy-done.3) | copy-start | bytes 638980
  77.5 33.1 %copy-start.6 = (bf16[2,4,384,64]{2,3,1,0:T(8,128)(2,1)S(1)}, bf16[2,4,384,64]{2,3,1,0:T(8,128)(2,1)}, u32[]{:S(2)}) copy-start(bf16[2,4,384,64]{2,3,1,0:T(8,128)(2,1)} %copy-done.5) | copy-start | bytes 1179652
  77.5 33.1 %copy-start.11 = (bf16[4,32,2,64]{1,3,0,2:T(8,128)(2,1)S(1)}, bf16[4,32,2,64]{1,3,0,2:T(8,128)(2,1)}, u32[]{:S(2)}) copy-start(bf16[4,32,2,64]{1,3,0,2:T(8,128)(2,1)} %copy-done.10) | copy-start | bytes 98308
  91.5 23.6 %all-to-all-start.2 = ((bf16[64,2,1,2048]{3,1,2,0:T(2,128)(2,1)}), bf16[64,2,1,2048]{3,1,2,0:T(2,128)(2,1)S(1)}, u32[]{:S(2)}, u32[]{:S(2)}) async-start(bf16[64,2,1,2048]{3,1,2,0:T(2,128)(2,1)} %bitcast.24), calls=%async_computation.2 | async-start | bytes 1048576 | tf_op jit(solution)/shard_map/all_to_all | solution.py:166
  111.1 3.9 %copy-start.9 = (bf16[128,128]{1,0:T(8,128)(2,1)}, bf16[128,128]{1,0:T(8,128)(2,1)S(1)}, u32[]{:S(2)}) copy-start(bf16[128,128]{1,0:T(8,128)(2,1)S(1)} %convert_element_type.82) | copy-start | bytes 98308
  115.0 29.8 %all-to-all-start.3 = ((bf16[64,32,128]{2,1,0:T(8,128)(2,1)}), bf16[64,32,128]{2,1,0:T(8,128)(2,1)S(1)}, u32[]{:S(2)}, u32[]{:S(2)}) async-start(bf16[64,32,128]{2,1,0:T(8,128)(2,1)} %bitcast.30), calls=%async_computation.3 | async-start | bytes 1048576 | tf_op jit(solution)/shard_map/all_to_all | solution.py:34
where the time goes:
time: 146 us
  waiting for transfers between devices  56.8 us (39%)
  starting transfers between devices  39.4 us (27%)
  local copies, waits for them, and re-layouts  22.7 us (16%)
  blocking collectives  13.5 us (9%)
  other arithmetic  8.99 us (6%)
  matrix products  2.89 us (2%)
    all_to_all x1, waiting for transfers between devices, sent_together(): lax.all_to_all(both, axis, split_axis=split_dim, concat_axis=concat_dim,...  27.8 us
    all_to_all x1, starting transfers between devices, sent_together(): lax.all_to_all(both, axis, split_axis=split_dim, concat_axis=concat_dim,...  16.7 us
    all_to_all x1, waiting for transfers between devices, sum_at_owner(): lax.all_to_all(tiles, axis, split_axis=0, concat_axis=0, tiled=True)  13.6 us
    all_gather x1, blocking collectives, body(): whole_input = lax.all_gather(normed_input, 'tp', axis=1, tiled=True)  13.5 us
    all_to_all x1, waiting for transfers between devices, body(): lax.all_to_all(to_slots(key_grad).astype(jnp.bfloat16), 'kv', split_axis=...  12.8 us
    all_to_all x1, starting transfers between devices, sum_at_owner(): lax.all_to_all(tiles, axis, split_axis=0, concat_axis=0, tiled=True)  10.1 us
    all_to_all x1, starting transfers between devices, body(): lax.all_to_all(to_slots(key_grad).astype(jnp.bfloat16), 'kv', split_axis=...  7.14 us
    all_to_all x1, starting transfers between devices, body(): lax.all_to_all(to_slots(value_grad).astype(jnp.bfloat16), 'kv', split_axi...  5.45 us
  transfers between devices with their start and end apart: 4, of which 4 were waited for; matrix products, arithmetic and copies ran while one was open for 10% of the time, Pallas kernels for 0%

commit v1 on v0

--- a/solution.py
+++ b/solution.py
@@ -8,6 +8,28 @@
 SEL = 12
 MOST = 1
 MASKED = -1e30
+
+
+def in_order(blocks, dim):
+    shape = list(blocks.shape[1:])
+    shape[dim] *= blocks.shape[0]
+    return jnp.moveaxis(blocks, 0, dim).reshape(shape)
+
+
+def collect(shard, axis, dim):
+    peers = lax.axis_size(axis)
+    pairs = [(i, (i + 1) % peers) for i in range(peers)]
+    back = [(b, a) for a, b in pairs]
+    lower, upper = ([], [])
+    for step in range(peers - 1):
+        if step % 2 == 0:
+            lower.append(lax.ppermute(lower[-1] if lower else shard, axis, pairs))
+        else:
+            upper.append(lax.ppermute(upper[-1] if upper else shard, axis, back))
+    parts = jnp.stack([*lower[::-1], shard, *upper])
+    shift = lax.axis_index(axis) - len(lower)
+    parts = parts[(jnp.arange(peers) - shift) % peers]
+    return in_order(parts, dim)
 
 
 def sent_together(arrays, axis, split_dim, concat_dim, along):
@@ -182,7 +204,7 @@
 
     grad_keys = settle(back_keys, key_grad)
     grad_values = settle(back_values, value_grad)
-    whole_input = lax.all_gather(normed_input, "tp", axis=1, tiled=True)
+    whole_input = collect(normed_input, "tp", 1)
     grad_weight = sum_at_owner(
         lax.dot_general(
             whole_input, grad_queries, (((0,), (0,)), ((), ())), preferred_element_type=jnp.float32

time: 146 us -> 141 us (0.966)
  the two profiles are of different devices: /device:TPU:8 before, /device:TPU:6 now
where the time goes in v1:
time: 141 us; the launch traced here: 140 us
  waiting for transfers between devices  57.8 us (41%)
  starting transfers between devices  39.6 us (28%)
  local copies, waits for them, and re-layouts  27.3 us (19%)
  other arithmetic  9.05 us (6%)
  matrix products  4.65 us (3%)
  between operations  1.45 us (1%)
    all_to_all x1, starting transfers between devices, sent_together(): lax.all_to_all(both, axis, split_axis=split_dim, concat_axis=concat_dim,...  16.9 us
    all_to_all x1, waiting for transfers between devices, sent_together(): lax.all_to_all(both, axis, split_axis=split_dim, concat_axis=concat_dim,...  14.1 us
    all_to_all x1, waiting for transfers between devices, body(): lax.all_to_all(to_slots(value_grad).astype(jnp.bfloat16), 'kv', split_axi...  13.3 us
    all_to_all x1, waiting for transfers between devices, sum_at_owner(): lax.all_to_all(tiles, axis, split_axis=0, concat_axis=0, tiled=True)  12.1 us
    all_to_all x1, waiting for transfers between devices, body(): lax.all_to_all(to_slots(key_grad).astype(jnp.bfloat16), 'kv', split_axis=...  10.4 us
    ppermute x4, waiting for transfers between devices, collect(): lower.append(lax.ppermute(lower[-1] if lower else shard, axis, pairs))  7.8 us
    all_to_all x1, starting transfers between devices, body(): lax.all_to_all(to_slots(key_grad).astype(jnp.bfloat16), 'kv', split_axis=...  6.75 us
    unnamed x58, local copies, waits for them, and re-layouts  6.36 us
  transfers between devices with their start and end apart: 11, of which 8 were waited for; matrix products, arithmetic and copies ran while one was open for 22% of the time, Pallas kernels for 0%

profile of v1, /device:TPU:6, one launch (start us, length us, event | category | flops | bytes accessed | tf_op | source)
XLA Modules:
  0.0 139.8 jit_solution(4081483890278886516)
XLA Ops:
  0.7 0.9 copy.97
  2.7 0.8 reshape.266
  4.3 0.9 gather_fusion.1
  5.2 0.9 gather_fusion.2
  7.0 2.1 %pad_maximum_fusion = bf16[64,4,1,2048]{3,1,2,0:T(4,128)(2,1)} fusion(bf16[64,2,1,2048]{3,1,2,0:T(2,128)(2,1)S(1)} %bitcast.121, bf16[64,2,1,2048]{3,1,2,0:T(2,128)(2,1)S(1)} %bitcast.122), kind=kLoop, calls=%fused_computation.18 | loop fusion | flops 2097152 | bytes 2097152 | tf_op jit(solution)/shard_map/concatenate | solution.py:36
  9.1 16.9 %all-to-all-start = ((bf16[64,4,1,2048]{3,1,2,0:T(4,128)(2,1)}), bf16[64,4,1,2048]{3,1,2,0:T(4,128)(2,1)S(1)}, u32[]{:S(2)}, u32[]{:S(2)}) async-start(bf16[64,4,1,2048]{3,1,2,0:T(4,128)(2,1)} %pad_maximum_fusion), calls=%async_computation | async-start | bytes 2097152 | tf_op jit(solution)/shard_map/all_to_all | solution.py:38
  26.1 1.7 %collective-permute-start.4 = (bf16[128,256]{1,0:T(8,128)(2,1)S(1)}, bf16[128,256]{1,0:T(8,128)(2,1)S(1)}, u32[]{:S(2)}, u32[]{:S(2)}) collective-permute-start(bf16[128,256]{1,0:T(8,128)(2,1)S(1)} %copy-done.12), channel_id=1, source_target_pairs={{1,0},{2,1},{3,2},{4,3},{5,4},{6,5},{7,6},{0,7},{9,8},{10,9},{11,1... | collective-permute-start | bytes 196616 | tf_op jit(solution)/shard_map/ppermute | solution.py:28
  29.1 0.6 collective-permute-done
  29.7 3.7 %collective-permute-done.1 = bf16[128,256]{1,0:T(8,128)(2,1)S(1)} collective-permute-done((bf16[128,256]{1,0:T(8,128)(2,1)S(1)}, bf16[128,256]{1,0:T(8,128)(2,1)S(1)}, u32[]{:S(2)}, u32[]{:S(2)}) %collective-permute-start.1) | collective-permute-done | bytes 65568 | tf_op jit(solution)/shard_map/ppermute | solution.py:26
  33.5 1.8 %collective-permute-start.5 = (bf16[128,256]{1,0:T(8,128)(2,1)S(1)}, bf16[128,256]{1,0:T(8,128)(2,1)}, u32[]{:S(2)}, u32[]{:S(2)}) collective-permute-start(bf16[128,256]{1,0:T(8,128)(2,1)S(1)} %collective-permute-done.4), channel_id=1, source_target_pairs={{1,0},{2,1},{3,2},{4,3},{5,4},{6,5},{7,6},{0,7},{9,8},{10,9},{11,1... | collective-permute-start | bytes 196616 | tf_op jit(solution)/shard_map/ppermute | solution.py:28
  35.2 1.9 %collective-permute-done.2 = bf16[128,256]{1,0:T(8,128)(2,1)S(1)} collective-permute-done((bf16[128,256]{1,0:T(8,128)(2,1)S(1)}, bf16[128,256]{1,0:T(8,128)(2,1)S(1)}, u32[]{:S(2)}, u32[]{:S(2)}) %collective-permute-start.2) | collective-permute-done | bytes 65568 | tf_op jit(solution)/shard_map/ppermute | solution.py:26
  37.1 0.7 collective-permute-start.3
  37.8 1.4 %collective-permute-start.6 = (bf16[128,256]{1,0:T(8,128)(2,1)}, bf16[128,256]{1,0:T(8,128)(2,1)}, u32[]{:S(2)}, u32[]{:S(2)}) collective-permute-start(bf16[128,256]{1,0:T(8,128)(2,1)} %collective-permute-done.5), channel_id=1, source_target_pairs={{1,0},{2,1},{3,2},{4,3},{5,4},{6,5},{7,6},{0,7},{9,8},{10,9},{11,1... | collective-permute-start | bytes 196616 | tf_op jit(solution)/shard_map/ppermute | solution.py:28
  39.2 1.6 %collective-permute-done.3 = bf16[128,256]{1,0:T(8,128)(2,1)S(1)} collective-permute-done((bf16[128,256]{1,0:T(8,128)(2,1)S(1)}, bf16[128,256]{1,0:T(8,128)(2,1)S(1)}, u32[]{:S(2)}, u32[]{:S(2)}) %collective-permute-start.3) | collective-permute-done | bytes 65568 | tf_op jit(solution)/shard_map/ppermute | solution.py:26
  40.8 0.6 bitcast_dynamic-update-slice_fusion.7
  41.4 14.1 %all-to-all-done = bf16[64,4,1,2048]{3,1,2,0:T(4,128)(2,1)S(1)} async-done(((bf16[64,4,1,2048]{3,1,2,0:T(4,128)(2,1)}), bf16[64,4,1,2048]{3,1,2,0:T(4,128)(2,1)S(1)}, u32[]{:S(2)}, u32[]{:S(2)}) %all-to-all-start) | async-done | bytes 1048608 | tf_op jit(solution)/shard_map/all_to_all | solution.py:38
  55.6 0.7 fusion.47
  56.8 0.8 gather_fusion.4
  57.6 0.8 gather_fusion.3
  58.6 0.8 reshape.279
  59.7 0.8 reshape.275
  63.4 2.0 %scatter_custom_fusion = f32[128,2048]{1,0:T(8,128)S(1)} fusion(s32[96]{0:T(128)S(1)} %reshape.274, f32[96,2048]{1,0:T(8,128)S(1)} %reshape.332, f32[]{:T(128)} %constant.121.clone.1), kind=kCustom, calls=%fused_computation.26 | custom fusion | flops 196608 | bytes 1048580 | tf_op jit(solution)/shard_map/scatter-add | solution.py:179
  65.6 1.1 convert_element_type.83
  66.7 6.7 %all-to-all-start.1 = ((bf16[64,2,1,2048]{3,1,2,0:T(2,128)(2,1)}), bf16[64,2,1,2048]{3,1,2,0:T(2,128)(2,1)}, u32[]{:S(2)}, u32[]{:S(2)}) async-start(bf16[64,2,1,2048]{3,1,2,0:T(2,128)(2,1)} %bitcast.18), calls=%async_computation.1 | async-start | bytes 1048576 | tf_op jit(solution)/shard_map/all_to_all | solution.py:185
  73.5 0.6 bitcast_dynamic-update-slice_fusion.6
  74.1 0.6 bitcast_dynamic-update-slice_fusion.5
  74.7 0.6 bitcast_dynamic-update-slice_fusion.4
  75.4 0.6 bitcast_dynamic-update-slice_fusion.3
  76.4 1.0 copy-done
  78.4 2.0 %scatter_custom_fusion.1 = f32[128,2048]{1,0:T(8,128)S(1)} fusion(s32[96]{0:T(128)S(1)} %reshape.274, f32[96,2048]{1,0:T(8,128)S(1)} %reshape.340, f32[]{:T(128)} %constant.121.clone.1), kind=kCustom, calls=%fused_computation.24 | custom fusion | flops 196608 | bytes 1048580 | tf_op jit(solution)/shard_map/scatter-add | solution.py:179
  80.5 1.1 convert_element_type.89
  81.7 10.4 %all-to-all-done.1 = bf16[64,2,1,2048]{3,1,2,0:T(2,128)(2,1)} async-done(((bf16[64,2,1,2048]{3,1,2,0:T(2,128)(2,1)}), bf16[64,2,1,2048]{3,1,2,0:T(2,128)(2,1)}, u32[]{:S(2)}, u32[]{:S(2)}) %all-to-all-start.1) | async-done | bytes 524320 | tf_op jit(solution)/shard_map/all_to_all | solution.py:185
  92.1 5.3 %all-to-all-start.2 = ((bf16[64,2,1,2048]{3,1,2,0:T(2,128)(2,1)}), bf16[64,2,1,2048]{3,1,2,0:T(2,128)(2,1)S(1)}, u32[]{:S(2)}, u32[]{:S(2)}) async-start(bf16[64,2,1,2048]{3,1,2,0:T(2,128)(2,1)} %bitcast.24), calls=%async_computation.2 | async-start | bytes 1048576 | tf_op jit(solution)/shard_map/all_to_all | solution.py:188
  97.4 0.8 bitcast_dynamic-update-slice_fusion.1
  98.3 0.8 bitcast_dynamic-update-slice_fusion
  99.1 0.6 gather_fusion
  100.0 1.3 fusion.5
  101.5 1.1 convolution_convert_fusion
  102.5 13.3 %all-to-all-done.2 = bf16[64,2,1,2048]{3,1,2,0:T(2,128)(2,1)S(1)} async-done(((bf16[64,2,1,2048]{3,1,2,0:T(2,128)(2,1)}), bf16[64,2,1,2048]{3,1,2,0:T(2,128)(2,1)S(1)}, u32[]{:S(2)}, u32[]{:S(2)}) %all-to-all-start.2) | async-done | bytes 524320 | tf_op jit(solution)/shard_map/all_to_all | solution.py:188
  115.8 5.0 %all-to-all-start.3 = ((bf16[64,32,128]{2,1,0:T(8,128)(2,1)}), bf16[64,32,128]{2,1,0:T(8,128)(2,1)S(1)}, u32[]{:S(2)}, u32[]{:S(2)}) async-start(bf16[64,32,128]{2,1,0:T(8,128)(2,1)} %bitcast.40), calls=%async_computation.3 | async-start | bytes 1048576 | tf_op jit(solution)/shard_map/all_to_all | solution.py:56
  120.9 1.2 reshape.283
  122.4 0.5 fusion.30
  123.3 0.7 convert_element_type.86
  124.4 0.5 fusion.28
  125.1 1.0 fusion.18
  126.2 0.7 convert_element_type.92
  127.0 12.1 %all-to-all-done.3 = bf16[64,32,128]{2,1,0:T(8,128)(2,1)S(1)} async-done(((bf16[64,32,128]{2,1,0:T(8,128)(2,1)}), bf16[64,32,128]{2,1,0:T(8,128)(2,1)S(1)}, u32[]{:S(2)}, u32[]{:S(2)}) %all-to-all-start.3) | async-done | bytes 524320 | tf_op jit(solution)/shard_map/all_to_all | solution.py:56
  139.1 0.7 convert_reduce_fusion
  (133 shorter events, 10.9 us)
Async XLA Ops:
  0.6 3.0 %copy-start.21 = (s32[2,256,12]{1,0,2:T(2,128)S(1)}, s32[2,256,12]{1,0,2:T(2,128)}, u32[]{:S(2)}) copy-start(s32[2,256,12]{1,0,2:T(2,128)} %param.16) | copy-start | bytes 73732
  0.6 3.4 %copy-start.7 = (bf16[128,128]{1,0:T(8,128)(2,1)S(1)}, bf16[128,128]{1,0:T(8,128)(2,1)}, u32[]{:S(2)}) copy-start(bf16[128,128]{1,0:T(8,128)(2,1)} %param.13) | copy-start | bytes 98308
  9.1 16.9 %copy-start.12 = (bf16[128,256]{1,0:T(8,128)(2,1)S(1)}, bf16[128,256]{1,0:T(8,128)(2,1)}, u32[]{:S(2)}) copy-start(bf16[128,256]{1,0:T(8,128)(2,1)} %param.17) | copy-start | bytes 196612
  9.1 18.8 %copy-start.8 = (bf16[128,128]{1,0:T(8,128)(2,1)S(1)}, bf16[128,128]{1,0:T(8,128)(2,1)}, u32[]{:S(2)}) copy-start(bf16[128,128]{1,0:T(8,128)(2,1)} %param.12) | copy-start | bytes 98308
  9.1 19.0 %copy-start.22 = (bf16[128,128]{1,0:T(8,128)(2,1)S(1)}, bf16[128,128]{1,0:T(8,128)(2,1)}, u32[]{:S(2)}) copy-start(bf16[128,128]{1,0:T(8,128)(2,1)} %param.14) | copy-start | bytes 98308
  9.1 19.1 %copy-start.24 = (f32[2,128]{1,0:T(2,128)S(1)}, f32[2,128]{1,0:T(2,128)}, u32[]{:S(2)}) copy-start(f32[2,128]{1,0:T(2,128)} %param.15) | copy-start | bytes 3076
  9.1 19.4 %copy-start.23 = (bf16[128,128]{1,0:T(8,128)(2,1)S(1)}, bf16[128,128]{1,0:T(8,128)(2,1)}, u32[]{:S(2)}) copy-start(bf16[128,128]{1,0:T(8,128)(2,1)} %param.11) | copy-start | bytes 98308
  9.1 46.5 %all-to-all-start = ((bf16[64,4,1,2048]{3,1,2,0:T(4,128)(2,1)}), bf16[64,4,1,2048]{3,1,2,0:T(4,128)(2,1)S(1)}, u32[]{:S(2)}, u32[]{:S(2)}) async-start(bf16[64,4,1,2048]{3,1,2,0:T(4,128)(2,1)} %pad_maximum_fusion), calls=%async_computation | async-start | bytes 2097152 | tf_op jit(solution)/shard_map/all_to_all | solution.py:38
  26.0 3.7 %collective-permute-start = (bf16[128,256]{1,0:T(8,128)(2,1)S(1)}, bf16[128,256]{1,0:T(8,128)(2,1)S(1)}, u32[]{:S(2)}, u32[]{:S(2)}) collective-permute-start(bf16[128,256]{1,0:T(8,128)(2,1)S(1)} %copy-done.12), channel_id=1, source_target_pairs={{0,1},{1,2},{2,3},{3,4},{4,5},{5,6},{6,7},{7,0},{8,9},{9,10},{10,1... | collective-permute-start | bytes 196616 | tf_op jit(solution)/shard_map/ppermute | solution.py:26
  26.1 7.4 %collective-permute-start.4 = (bf16[128,256]{1,0:T(8,128)(2,1)S(1)}, bf16[128,256]{1,0:T(8,128)(2,1)S(1)}, u32[]{:S(2)}, u32[]{:S(2)}) collective-permute-start(bf16[128,256]{1,0:T(8,128)(2,1)S(1)} %copy-done.12), channel_id=1, source_target_pairs={{1,0},{2,1},{3,2},{4,3},{5,4},{6,5},{7,6},{0,7},{9,8},{10,9},{11,1... | collective-permute-start | bytes 196616 | tf_op jit(solution)/shard_map/ppermute | solution.py:28
  28.5 32.7 %copy-start.10 = (bf16[4,32,2,64]{1,3,0,2:T(8,128)(2,1)}, bf16[4,32,2,64]{1,3,0,2:T(8,128)(2,1)S(1)}, u32[]{:S(2)}) copy-start(bf16[4,32,2,64]{1,3,0,2:T(8,128)(2,1)S(1)} %copy.105) | copy-start | bytes 98308
  29.7 26.8 %copy-start.15 = (bf16[128,256]{1,0:T(8,128)(2,1)}, bf16[128,256]{1,0:T(8,128)(2,1)S(1)}, u32[]{:S(2)}) copy-start(bf16[128,256]{1,0:T(8,128)(2,1)S(1)} %collective-permute-done) | copy-start | bytes 196612
  29.7 3.7 %collective-permute-start.1 = (bf16[128,256]{1,0:T(8,128)(2,1)S(1)}, bf16[128,256]{1,0:T(8,128)(2,1)S(1)}, u32[]{:S(2)}, u32[]{:S(2)}) collective-permute-start(bf16[128,256]{1,0:T(8,128)(2,1)S(1)} %collective-permute-done), channel_id=1, source_target_pairs={{0,1},{1,2},{2,3},{3,4},{4,5},{5,6},{6,7},{7,0},{8,9},{9,10},{10,1... | collective-permute-start | bytes 196616 | tf_op jit(solution)/shard_map/ppermute | solution.py:26
  33.4 23.1 %copy-start.17 = (bf16[128,256]{1,0:T(8,128)(2,1)}, bf16[128,256]{1,0:T(8,128)(2,1)S(1)}, u32[]{:S(2)}) copy-start(bf16[128,256]{1,0:T(8,128)(2,1)S(1)} %collective-permute-done.1) | copy-start | bytes 196612
  33.4 3.7 %collective-permute-start.2 = (bf16[128,256]{1,0:T(8,128)(2,1)S(1)}, bf16[128,256]{1,0:T(8,128)(2,1)S(1)}, u32[]{:S(2)}, u32[]{:S(2)}) collective-permute-start(bf16[128,256]{1,0:T(8,128)(2,1)S(1)} %collective-permute-done.1), channel_id=1, source_target_pairs={{0,1},{1,2},{2,3},{3,4},{4,5},{5,6},{6,7},{7,0},{8,9},{9,10},{10,1... | collective-permute-start | bytes 196616 | tf_op jit(solution)/shard_map/ppermute | solution.py:26
  33.5 23.1 %copy-start.13 = (bf16[128,256]{1,0:T(8,128)(2,1)}, bf16[128,256]{1,0:T(8,128)(2,1)S(1)}, u32[]{:S(2)}) copy-start(bf16[128,256]{1,0:T(8,128)(2,1)S(1)} %collective-permute-done.4) | copy-start | bytes 196612
  33.5 4.3 %collective-permute-start.5 = (bf16[128,256]{1,0:T(8,128)(2,1)S(1)}, bf16[128,256]{1,0:T(8,128)(2,1)}, u32[]{:S(2)}, u32[]{:S(2)}) collective-permute-start(bf16[128,256]{1,0:T(8,128)(2,1)S(1)} %collective-permute-done.4), channel_id=1, source_target_pairs={{1,0},{2,1},{3,2},{4,3},{5,4},{6,5},{7,6},{0,7},{9,8},{10,9},{11,1... | collective-permute-start | bytes 196616 | tf_op jit(solution)/shard_map/ppermute | solution.py:28
  37.1 19.4 %copy-start.19 = (bf16[128,256]{1,0:T(8,128)(2,1)}, bf16[128,256]{1,0:T(8,128)(2,1)S(1)}, u32[]{:S(2)}) copy-start(bf16[128,256]{1,0:T(8,128)(2,1)S(1)} %collective-permute-done.2) | copy-start | bytes 196612
  37.1 3.7 %collective-permute-start.3 = (bf16[128,256]{1,0:T(8,128)(2,1)S(1)}, bf16[128,256]{1,0:T(8,128)(2,1)S(1)}, u32[]{:S(2)}, u32[]{:S(2)}) collective-permute-start(bf16[128,256]{1,0:T(8,128)(2,1)S(1)} %collective-permute-done.2), channel_id=1, source_target_pairs={{0,1},{1,2},{2,3},{3,4},{4,5},{5,6},{6,7},{7,0},{8,9},{9,10},{10,1... | collective-permute-start | bytes 196616 | tf_op jit(solution)/shard_map/ppermute | solution.py:26
  37.8 60.5 %collective-permute-start.6 = (bf16[128,256]{1,0:T(8,128)(2,1)}, bf16[128,256]{1,0:T(8,128)(2,1)}, u32[]{:S(2)}, u32[]{:S(2)}) collective-permute-start(bf16[128,256]{1,0:T(8,128)(2,1)} %collective-permute-done.5), channel_id=1, source_target_pairs={{1,0},{2,1},{3,2},{4,3},{5,4},{6,5},{7,6},{0,7},{9,8},{10,9},{11,1... | collective-permute-start | bytes 196616 | tf_op jit(solution)/shard_map/ppermute | solution.py:28
  60.8 1.2 copy-start.6
  61.5 0.8 copy-start.1
  61.6 0.7 copy-start.3
  65.4 8.0 %copy-start.20 = (bf16[128,256]{1,0:T(8,128)(2,1)S(1)}, bf16[128,256]{1,0:T(8,128)(2,1)}, u32[]{:S(2)}) copy-start(bf16[128,256]{1,0:T(8,128)(2,1)} %copy-done.19) | copy-start | bytes 196612
  65.5 8.7 %copy-start.18 = (bf16[128,256]{1,0:T(8,128)(2,1)S(1)}, bf16[128,256]{1,0:T(8,128)(2,1)}, u32[]{:S(2)}) copy-start(bf16[128,256]{1,0:T(8,128)(2,1)} %copy-done.17) | copy-start | bytes 196612
  65.5 9.2 %copy-start.16 = (bf16[128,256]{1,0:T(8,128)(2,1)S(1)}, bf16[128,256]{1,0:T(8,128)(2,1)}, u32[]{:S(2)}) copy-start(bf16[128,256]{1,0:T(8,128)(2,1)} %copy-done.15) | copy-start | bytes 196612
  65.5 10.5 %copy-start.2 = (f32[2,4,32,416]{3,2,1,0:T(8,128)S(1)}, f32[2,4,32,416]{3,2,1,0:T(8,128)}, u32[]{:S(2)}) copy-start(f32[2,4,32,416]{3,2,1,0:T(8,128)} %copy-done.1) | copy-start | bytes 1277956
  66.7 25.4 %all-to-all-start.1 = ((bf16[64,2,1,2048]{3,1,2,0:T(2,128)(2,1)}), bf16[64,2,1,2048]{3,1,2,0:T(2,128)(2,1)}, u32[]{:S(2)}, u32[]{:S(2)}) async-start(bf16[64,2,1,2048]{3,1,2,0:T(2,128)(2,1)} %bitcast.18), calls=%async_computation.1 | async-start | bytes 1048576 | tf_op jit(solution)/shard_map/all_to_all | solution.py:185
  76.4 1.0 copy-start
  80.4 17.0 %copy-start.5 = (bf16[8,128,256]{2,1,0:T(8,128)(2,1)S(1)}, bf16[8,128,256]{2,1,0:T(8,128)(2,1)}, u32[]{:S(2)}) copy-start(bf16[8,128,256]{2,1,0:T(8,128)(2,1)} %bitcast_dynamic-update-slice_fusion.3) | copy-start | bytes 1572868
  80.5 16.9 %copy-start.14 = (bf16[128,256]{1,0:T(8,128)(2,1)S(1)}, bf16[128,256]{1,0:T(8,128)(2,1)}, u32[]{:S(2)}) copy-start(bf16[128,256]{1,0:T(8,128)(2,1)} %copy-done.13) | copy-start | bytes 196612
  92.1 7.9 %copy-start.4 = (bf16[2,4,32,416]{3,2,1,0:T(8,128)(2,1)S(1)}, bf16[2,4,32,416]{3,2,1,0:T(8,128)(2,1)}, u32[]{:S(2)}) copy-start(bf16[2,4,32,416]{3,2,1,0:T(8,128)(2,1)} %copy-done.3) | copy-start | bytes 638980
  92.1 7.9 %copy-start.11 = (bf16[4,32,2,64]{1,3,0,2:T(8,128)(2,1)S(1)}, bf16[4,32,2,64]{1,3,0,2:T(8,128)(2,1)}, u32[]{:S(2)}) copy-start(bf16[4,32,2,64]{1,3,0,2:T(8,128)(2,1)} %copy-done.10) | copy-start | bytes 98308
  92.1 23.7 %all-to-all-start.2 = ((bf16[64,2,1,2048]{3,1,2,0:T(2,128)(2,1)}), bf16[64,2,1,2048]{3,1,2,0:T(2,128)(2,1)S(1)}, u32[]{:S(2)}, u32[]{:S(2)}) async-start(bf16[64,2,1,2048]{3,1,2,0:T(2,128)(2,1)} %bitcast.24), calls=%async_computation.2 | async-start | bytes 1048576 | tf_op jit(solution)/shard_map/all_to_all | solution.py:188
  101.5 20.7 %copy-start.9 = (bf16[128,128]{1,0:T(8,128)(2,1)}, bf16[128,128]{1,0:T(8,128)(2,1)S(1)}, u32[]{:S(2)}) copy-start(bf16[128,128]{1,0:T(8,128)(2,1)S(1)} %convert_element_type.81) | copy-start | bytes 98308
  115.8 23.3 %all-to-all-start.3 = ((bf16[64,32,128]{2,1,0:T(8,128)(2,1)}), bf16[64,32,128]{2,1,0:T(8,128)(2,1)S(1)}, u32[]{:S(2)}, u32[]{:S(2)}) async-start(bf16[64,32,128]{2,1,0:T(8,128)(2,1)} %bitcast.40), calls=%async_computation.3 | async-start | bytes 1048576 | tf_op jit(solution)/shard_map/all_to_all | solution.py:56
